TPU v7x, 32 devices: a whole 2x2x4 slice. The times are simulated.
32 devices in a mesh: sp: 8 (over z, x), tp: 4 (over y, core).
Axes of the slice: x: 2, y: 2, z: 4, core: 2. Of those that a mesh axis runs over, the one named last changes fastest.
Arguments:
- tokens: bfloat16 [4096, 2048], P(('sp', 'tp')), may hold values from -8 to 8
- in_gain: float32 [2048], replicated, may hold values from 0.1 to 1.9
- w_conv_val: bfloat16 [2048, 1024], P('sp', 'tp'), may hold values from -0.125 to 0.125
- w_conv_gate: bfloat16 [2048, 1024], P('sp', 'tp'), may hold values from -0.125 to 0.125
- w_query: bfloat16 [2048, 1024], P('sp', 'tp'), may hold values from -1 to 1
- w_key: bfloat16 [2048, 256], P('sp', 'tp'), may hold values from -1 to 1
- value_weight: bfloat16 [2048, 256], P('sp', 'tp'), may hold values from -0.125 to 0.125
- conv_taps: float32 [31, 1024], P(None, 'tp'), may hold values from -1 to 1
- conv_bias: float32 [1024], P('tp'), may hold values from -3 to 3
- norm_gain: float32 [1024], P('tp'), may hold values from 0.1 to 1.9
- norm_bias: float32 [1024], P('tp'), may hold values from -3 to 3
- head_sink_logit: float32 [16], P('tp'), may hold values from 4 to 7
- w_out_conv: bfloat16 [1024, 2048], P('tp', 'sp'), may hold values from -0.125 to 0.125
- w_out_attn: bfloat16 [1024, 2048], P('tp', 'sp'), may hold values from -0.125 to 0.125
Outputs:
- mixed: bfloat16 [4096, 2048], P(('sp', 'tp'))
- log_total: float32 [4096, 16], P('sp', 'tp')
All inputs are finite; a program needn't handle non-finite values.
Results may differ from a plain program's by a relative error of at most 0.012.
Values may be sent and summed in bfloat16 or wider, within the bound.
A program may use at most 64 MiB of HBM per device.

v0:
```python
import jax
import jax.numpy as jnp
from jax import lax
from jax.sharding import PartitionSpec as P

WINDOW_REACH = 128


def with_halo(cells, sides, width):
    for axis, dim in sides:
        count = lax.axis_size(axis)
        ends = count - 1
        head = lax.slice_in_dim(cells, 0, width, axis=dim)
        tail = lax.slice_in_dim(cells, cells.shape[dim] - width, cells.shape[dim], axis=dim)
        cells = jnp.concatenate(
            [
                lax.ppermute(tail, axis, [(i, (i + 1) % count) for i in range(ends)]),
                cells,
                lax.ppermute(head, axis, [((i + 1) % count, i) for i in range(ends)]),
            ],
            axis=dim,
        )
    return cells


def on_device(
    tokens,
    in_gain,
    w_conv_val,
    w_conv_gate,
    w_query,
    w_key,
    value_weight,
    conv_taps,
    conv_bias,
    norm_gain,
    norm_bias,
    head_sink_logit,
    w_out_conv,
    w_out_attn,
):
    flt = tokens.astype(jnp.float32)
    normed = (
        flt * lax.rsqrt(jnp.mean(flt * flt, axis=-1, keepdims=True) + 1e-06) * in_gain
    ).astype(jnp.bfloat16)
    val_full, gate_full, query_full, key_full, value_full = (
        lax.all_gather(w_conv_val, "sp", axis=0, tiled=True),
        lax.all_gather(w_conv_gate, "sp", axis=0, tiled=True),
        lax.all_gather(w_query, "sp", axis=0, tiled=True),
        lax.all_gather(w_key, "sp", axis=0, tiled=True),
        lax.all_gather(value_weight, "sp", axis=0, tiled=True),
    )
    joined = jnp.concatenate([val_full, gate_full, query_full, key_full, value_full], axis=1)
    projected = jnp.dot(
        lax.all_gather(normed, "tp", axis=0, tiled=True), joined, preferred_element_type=jnp.float32
    )
    chans = val_full.shape[1]
    qwidth = query_full.shape[1]
    kwidth = key_full.shape[1]
    length = projected.shape[0]
    glu = (projected[:, :chans] * jax.nn.sigmoid(projected[:, chans : 2 * chans])).astype(
        jnp.bfloat16
    )
    base = 2 * chans
    query_matrix = projected[:, base : base + qwidth].astype(jnp.bfloat16)
    key = projected[:, base + qwidth : base + qwidth + kwidth].astype(jnp.bfloat16)
    value_matrix = projected[:, base + qwidth + kwidth :].astype(jnp.bfloat16)
    taps = conv_taps.shape[0]
    half = taps // 2
    padded = with_halo(glu, (("sp", 0),), half)
    filtered = jnp.zeros(glu.shape, jnp.float32) + conv_bias
    for offset in range(taps):
        filtered = (
            filtered + padded[offset : offset + length].astype(jnp.float32) * conv_taps[offset]
        )
    sums, squares = lax.psum(
        (jnp.sum(filtered, axis=-1), jnp.sum(filtered * filtered, axis=-1)), "tp"
    )
    count = chans * lax.axis_size("tp")
    center = (sums / count)[:, None]
    spread = (squares / count)[:, None] - center * center
    conv_out = jax.nn.silu(
        (filtered - center) * lax.rsqrt(spread + 1e-05) * norm_gain + norm_bias
    ).astype(jnp.bfloat16)
    heads_here = head_sink_logit.shape[0]
    head_size = qwidth // heads_here
    kv_here = kwidth // head_size
    query_groups = heads_here // kv_here
    stacked = jnp.stack([key, value_matrix], axis=0)
    banded = with_halo(stacked, (("sp", 1),), WINDOW_REACH)
    span = length + 2 * WINDOW_REACH
    key_band = banded[0].reshape(span, kv_here, head_size)
    value_band = banded[1].reshape(span, kv_here, head_size)
    query4_grouped = query_matrix.reshape(length, kv_here, query_groups, head_size)
    scores = jnp.einsum(
        "qkgd,jkd->kgqj", query4_grouped, key_band, preferred_element_type=jnp.float32
    ) * head_size ** (-0.5)
    offset_pos = lax.axis_index("sp") * length
    seq_len = length * lax.axis_size("sp")
    qpos = offset_pos + jnp.arange(length, dtype=jnp.int32)
    kpos = offset_pos - WINDOW_REACH + jnp.arange(span, dtype=jnp.int32)
    valid = (
        (jnp.abs(qpos[:, None] - kpos[None, :]) <= WINDOW_REACH)
        & (kpos[None, :] >= 0)
        & (kpos[None, :] < seq_len)
    )
    sink_column = head_sink_logit.reshape(kv_here, query_groups, 1)
    masked = jnp.where(valid, scores, -1e30)
    top = jnp.maximum(jnp.max(masked, axis=-1), sink_column)
    expd = jnp.where(valid, jnp.exp(masked - top[..., None]), 0.0)
    total = jnp.sum(expd, axis=-1) + jnp.exp(sink_column - top)
    probs = (expd / total[..., None]).astype(jnp.bfloat16)
    attended = jnp.einsum(
        "kgqj,jkd->qkgd", probs, value_band, preferred_element_type=jnp.float32
    ).astype(jnp.bfloat16)
    attended = attended.reshape(length, qwidth)
    log_total = (top + jnp.log(total)).reshape(heads_here, length).T
    out_conv_cols, out_attn_cols = (
        lax.all_gather(w_out_conv, "sp", axis=1, tiled=True),
        lax.all_gather(w_out_attn, "sp", axis=1, tiled=True),
    )
    out_rows = jnp.concatenate([out_conv_cols, out_attn_cols], axis=0)
    features = jnp.concatenate([conv_out, attended], axis=1)
    mixed = lax.psum_scatter(
        jnp.dot(features, out_rows, preferred_element_type=jnp.float32).astype(jnp.bfloat16),
        "tp",
        scatter_dimension=0,
        tiled=True,
    )
    return (mixed, log_total)


def solution(mesh):
    return jax.shard_map(
        on_device,
        mesh=mesh,
        in_specs=(
            P(("sp", "tp"), None),
            P(),
            P("sp", "tp"),
            P("sp", "tp"),
            P("sp", "tp"),
            P("sp", "tp"),
            P("sp", "tp"),
            P(None, "tp"),
            P("tp"),
            P("tp"),
            P("tp"),
            P("tp"),
            P("tp", "sp"),
            P("tp", "sp"),
        ),
        out_specs=(P(("sp", "tp"), None), P("sp", "tp")),
        check_vma=False,
    )
```

profile of v0, /device:TPU:0, one launch (start us, length us, event | category | flops | bytes accessed | tf_op | source)
XLA Modules:
  0.0 283.3 jit_solution(18106258982470907341)
XLA Ops:
  7.2 0.0 all-gather.11.cloned.1.call-start
  7.2 0.7 all-gather.11.cloned.1.call-update
  7.9 0.0 all-gather.13.cloned.1.call-start
  7.9 0.7 all-gather.13.cloned.1.call-update
  8.6 0.0 all-gather.9.cloned.1.call-start
  8.7 0.7 all-gather.9.cloned.1.call-update
  9.4 0.0 all-gather.7.cloned.1.call-start
  9.4 1.2 fusion.12
  10.7 2.0 fusion.14
  12.7 0.0 all-gather.15.cloned.1.call-start
  12.8 0.5 all-gather.15.cloned.1.call-update
  13.3 0.0 all-gather.17.cloned.1.call-start
  13.4 0.5 all-gather.17.cloned.1.call-update
  13.9 0.0 reduce-scatter.2.cloned.1.call-start
  13.9 1.0 fusion.63
  15.0 1.0 fusion.64
  16.0 33.1 %all_gather.28 = bf16[2048,64]{0,1:T(8,128)(2,1)S(1)} all-gather(bf16[256,64]{0,1:T(8,128)(2,1)} %param.19), channel_id=1, replica_groups=mesh['sp'=8,'tp'=4] {'sp'}, dimensions={0}, use_global_device_ids=true | all-gather | bytes 294912 | tf_op jit(solution)/shard_map/all_gather | solution.py:50
  49.1 0.3 copy.23
  49.4 31.1 %all_gather.29 = bf16[2048,64]{0,1:T(8,128)(2,1)S(1)} all-gather(bf16[256,64]{0,1:T(8,128)(2,1)} %param.20), channel_id=1, replica_groups=mesh['sp'=8,'tp'=4] {'sp'}, dimensions={0}, use_global_device_ids=true | all-gather | bytes 294912 | tf_op jit(solution)/shard_map/all_gather | solution.py:51
  80.5 0.3 copy.24
  80.8 0.8 fusion.8
  81.6 14.2 %all-gather.13.cloned.1.call-done = bf16[2048,256]{1,0:T(8,128)(2,1)} async-done(((bf16[256,256]{1,0:T(8,128)(2,1)}), bf16[2048,256]{1,0:T(8,128)(2,1)}) %all-gather.13.cloned.1.call-update) | async-done | bytes 1048592 | tf_op jit(solution)/shard_map/all_gather | solution.py:49
  95.8 41.2 %all-gather.9.cloned.1.call-done = bf16[2048,256]{1,0:T(8,128)(2,1)} async-done(((bf16[256,256]{1,0:T(8,128)(2,1)}), bf16[2048,256]{1,0:T(8,128)(2,1)}) %all-gather.9.cloned.1.call-update) | async-done | bytes 1048592 | tf_op jit(solution)/shard_map/all_gather | solution.py:47
  136.9 6.6 %concatenate.47 = bf16[2048,896]{1,0:T(8,128)(2,1)} concatenate(bf16[2048,256]{1,0:T(8,128)(2,1)} %all-gather.9.cloned.1.call-done, bf16[2048,256]{1,0:T(8,128)(2,1)} %all-gather.11.cloned.1.call-done, bf16[2048,256]{1,0:T(8,128)(2,1)} %all-gather.13.cloned.1.call-done, bf16[2048,64]{1,0:T(8,128)(2,1)S(1)} %copy.23, bf16[2048,64]{1,0:T(8,128)(2,1)S(1)} %copy.24), dimensions={1} | concatenate | bytes 7340032 | tf_op jit(solution)/shard_map/concatenate | solution.py:53
  143.5 16.7 %all-gather.7.cloned.1.call-done = bf16[512,2048]{1,0:T(8,128)(2,1)} async-done(((bf16[128,2048]{1,0:T(8,128)(2,1)}), bf16[512,2048]{1,0:T(8,128)(2,1)}) %all-gather.7.cloned.1.call-update) | async-done | bytes 2097168 | tf_op jit(solution)/shard_map/all_gather | solution.py:55
  160.2 5.0 %fusion.65 = (bf16[512,896]{1,0:T(8,128)(2,1)S(1)}, f32[512,896]{1,0:T(8,128)S(1)}) fusion(bf16[512,2048]{1,0:T(8,128)(2,1)} %all-gather.7.cloned.1.call-done, bf16[2048,896]{1,0:T(8,128)(2,1)} %concatenate.47), kind=kOutput, calls=%fused_computation.136 | convolution fusion | flops 1879506944 | bytes 8519680 | tf_op jit(solution)/shard_map/dot_general | solution.py:54
  165.3 0.1 fusion.22
  165.4 3.4 %collective-permute-start = (bf16[15,256]{1,0:T(8,128)(2,1)S(1)}, bf16[15,256]{1,0:T(8,128)(2,1)S(1)}, u32[]{:S(2)}, u32[]{:S(2)}) collective-permute-start(bf16[15,256]{1,0:T(8,128)(2,1)S(1)} %get-tuple-element.9), channel_id=1, source_target_pairs={{0,4},{4,8},{8,12},{12,16},{16,20},{20,24},{24,28},{1,5},{5,9},{9,... | collective-permute-start | bytes 23048 | tf_op jit(solution)/shard_map/ppermute | solution.py:17
  168.8 1.3 collective-permute-start.1
  170.1 0.1 slice_bitcast_fusion.5
  170.3 4.5 %collective-permute-start.2 = (bf16[2,128,64]{2,1,0:T(8,128)(2,1)S(1)}, bf16[2,128,64]{2,1,0:T(8,128)(2,1)S(1)}, u32[]{:S(2)}, u32[]{:S(2)}) collective-permute-start(bf16[2,128,64]{2,1,0:T(8,128)(2,1)S(1)} %get-tuple-element.11), channel_id=1, source_target_pairs={{0,4},{4,8},{8,12},{12,16},{16,20},{20,24},{24,28},{1,5},{5,9},{9,... | collective-permute-start | bytes 98312 | tf_op jit(solution)/shard_map/ppermute | solution.py:17
  174.8 1.3 collective-permute-start.3
  176.1 0.1 copy.25
  176.3 2.8 fusion.61
  179.1 6.3 %all-reduce = (f32[512]{0:T(512)S(1)}, f32[512]{0:T(512)S(1)}) all-reduce(f32[512]{0:T(512)S(1)} %get-tuple-element.3, f32[512]{0:T(512)S(1)} %get-tuple-element.2), channel_id=1, replica_groups=mesh['sp'=8,'tp'=4] {'tp'}, use_global_device_ids=true, to_apply=%region_4.0 | all-reduce | flops 1024 | bytes 8192 | tf_op jit(solution)/shard_map/psum | solution.py:76
  185.4 0.3 multiply_convert_fusion
  185.7 0.1 pad_maximum_fusion
  185.7 1.1 fusion
  186.9 0.1 broadcast_maximum_fusion
  187.0 1.6 fusion.1
  188.5 0.1 exponential_add_fusion
  188.6 2.2 fusion.9
  190.8 0.1 copy.29
  191.0 10.6 %all-gather.15.cloned.1.call-done = bf16[256,2048]{1,0:T(8,128)(2,1)} async-done(((bf16[256,256]{1,0:T(8,128)(2,1)}), bf16[256,2048]{1,0:T(8,128)(2,1)}) %all-gather.15.cloned.1.call-update) | async-done | bytes 1048592 | tf_op jit(solution)/shard_map/all_gather | solution.py:119
  201.6 40.3 %all-gather.17.cloned.1.call-done = bf16[256,2048]{1,0:T(8,128)(2,1)} async-done(((bf16[256,256]{1,0:T(8,128)(2,1)}), bf16[256,2048]{1,0:T(8,128)(2,1)}) %all-gather.17.cloned.1.call-update) | async-done | bytes 1048592 | tf_op jit(solution)/shard_map/all_gather | solution.py:120
  241.9 4.2 %convolution_convert_fusion = bf16[512,2048]{1,0:T(8,128)(2,1)} fusion(bf16[256,2048]{1,0:T(8,128)(2,1)} %all-gather.17.cloned.1.call-done, bf16[256,2048]{1,0:T(8,128)(2,1)} %all-gather.15.cloned.1.call-done, bf16[512,256]{1,0:T(8,128)(2,1)S(1)} %copy.29, bf16[512,256]{1,0:T(8,128)(2,1)S(1)} %multiply_convert_fusion), kind=kOutput, calls=%fused_computation.7 | convolution fusion | flops 1080033280 | bytes 4718592 | tf_op jit(solution)/shard_map/dot_general | solution.py:125
  246.1 0.7 fusion.53
  246.8 29.6 %reduce-scatter.2.cloned.1.call-done = bf16[128,2048]{1,0:T(8,128)(2,1)} async-done(((bf16[512,2048]{1,0:T(8,128)(2,1)}), bf16[128,2048]{1,0:T(8,128)(2,1)}) %reduce-scatter.2.cloned.1.call-update) | async-done | bytes 524304 | tf_op jit(solution)/shard_map/reduce_scatter | solution.py:124
  (23 shorter events, 0.2 us)
Async XLA Ops:
  7.2 74.4 %all-gather.11.cloned.1.call-start = ((), (), s32[]{:S(2)}) async-start(), calls=%async_computation.3 | async-start | bytes 1179648 | tf_op jit(solution)/shard_map/all_gather | solution.py:48
  7.9 87.9 %all-gather.13.cloned.1.call-start = ((), (), s32[]{:S(2)}) async-start(), calls=%async_computation.4 | async-start | bytes 1179648 | tf_op jit(solution)/shard_map/all_gather | solution.py:49
  8.6 128.3 %all-gather.9.cloned.1.call-start = ((), (), s32[]{:S(2)}) async-start(), calls=%async_computation.2 | async-start | bytes 1179648 | tf_op jit(solution)/shard_map/all_gather | solution.py:47
  9.4 150.8 %all-gather.7.cloned.1.call-start = ((), (), s32[]{:S(2)}) async-start(), calls=%async_computation.1 | async-start | bytes 2621440 | tf_op jit(solution)/shard_map/all_gather | solution.py:55
  12.7 188.9 %all-gather.15.cloned.1.call-start = ((), (), s32[]{:S(2)}) async-start(), calls=%async_computation.5 | async-start | bytes 1179648 | tf_op jit(solution)/shard_map/all_gather | solution.py:119
  13.3 228.6 %all-gather.17.cloned.1.call-start = ((), (), s32[]{:S(2)}) async-start(), calls=%async_computation.6 | async-start | bytes 1179648 | tf_op jit(solution)/shard_map/all_gather | solution.py:120
  13.9 262.5 %reduce-scatter.2.cloned.1.call-start = ((), (), s32[]{:S(2)}) async-start(), calls=%async_computation.7 | async-start | bytes 2621440 | tf_op jit(solution)/shard_map/reduce_scatter | solution.py:124
  143.5 32.8 %copy-start.1 = (f32[256]{0:T(256)S(1)}, f32[256]{0:T(256)}, u32[]{:S(2)}) copy-start(f32[256]{0:T(256)} %param.22) | copy-start | bytes 3076
  165.2 20.1 %copy-start.2 = (f32[256]{0:T(256)S(1)}, f32[256]{0:T(256)}, u32[]{:S(2)}) copy-start(f32[256]{0:T(256)} %param.24) | copy-start | bytes 3076
  165.2 20.1 %copy-start.3 = (f32[256]{0:T(256)S(1)}, f32[256]{0:T(256)}, u32[]{:S(2)}) copy-start(f32[256]{0:T(256)} %param.23) | copy-start | bytes 3076
  165.4 10.9 %collective-permute-start = (bf16[15,256]{1,0:T(8,128)(2,1)S(1)}, bf16[15,256]{1,0:T(8,128)(2,1)S(1)}, u32[]{:S(2)}, u32[]{:S(2)}) collective-permute-start(bf16[15,256]{1,0:T(8,128)(2,1)S(1)} %get-tuple-element.9), channel_id=1, source_target_pairs={{0,4},{4,8},{8,12},{12,16},{16,20},{20,24},{24,28},{1,5},{5,9},{9,... | collective-permute-start | bytes 23048 | tf_op jit(solution)/shard_map/ppermute | solution.py:17
  168.8 7.5 %collective-permute-start.1 = (bf16[15,256]{1,0:T(8,128)(2,1)S(1)}, bf16[15,256]{1,0:T(8,128)(2,1)S(1)}, u32[]{:S(2)}, u32[]{:S(2)}) collective-permute-start(bf16[15,256]{1,0:T(8,128)(2,1)S(1)} %get-tuple-element.10), channel_id=1, source_target_pairs={{4,0},{8,4},{12,8},{16,12},{20,16},{24,20},{28,24},{5,1},{9,5},{13... | collective-permute-start | bytes 23048 | tf_op jit(solution)/shard_map/ppermute | solution.py:19
  170.3 15.4 %collective-permute-start.2 = (bf16[2,128,64]{2,1,0:T(8,128)(2,1)S(1)}, bf16[2,128,64]{2,1,0:T(8,128)(2,1)S(1)}, u32[]{:S(2)}, u32[]{:S(2)}) collective-permute-start(bf16[2,128,64]{2,1,0:T(8,128)(2,1)S(1)} %get-tuple-element.11), channel_id=1, source_target_pairs={{0,4},{4,8},{8,12},{12,16},{16,20},{20,24},{24,28},{1,5},{5,9},{9,... | collective-permute-start | bytes 98312 | tf_op jit(solution)/shard_map/ppermute | solution.py:17
  174.8 10.8 %collective-permute-start.3 = (bf16[2,128,64]{2,1,0:T(8,128)(2,1)S(1)}, bf16[2,128,64]{2,1,0:T(8,128)(2,1)S(1)}, u32[]{:S(2)}, u32[]{:S(2)}) collective-permute-start(bf16[2,128,64]{2,1,0:T(8,128)(2,1)S(1)} %get-tuple-element.12), channel_id=1, source_target_pairs={{4,0},{8,4},{12,8},{16,12},{20,16},{24,20},{28,24},{5,1},{9,5},{13... | collective-permute-start | bytes 98312 | tf_op jit(solution)/shard_map/ppermute | solution.py:19
  185.4 1.5 copy-start
Sparse Core Ops, SparseCore 0:
  10.1 43.6 all-gather.10
  56.0 39.7 all-gather.12
  97.9 38.9 all-gather.8
  138.9 21.2 all-gather.6
  162.1 39.4 all-gather.14
  203.5 38.3 all-gather.16
  246.2 30.1 reduce-scatter.1
where the time goes:
time: 284 us; the launch traced here: 283 us
  waiting for transfers between devices  156 us (55%)
  blocking collectives  70.5 us (25%)
  between operations  14.4 us (5%)
  matrix products  12.5 us (4%)
  starting transfers between devices  10.8 us (4%)
  other arithmetic  9.74 us (3%)
  local copies, waits for them, and re-layouts  9.6 us (3%)
    all_gather x1, waiting for transfers between devices, on_device(): lax.all_gather(w_conv_val, 'sp', axis=0, tiled=True)  41.2 us
    all_gather x1, waiting for transfers between devices, on_device(): lax.all_gather(w_out_attn, 'sp', axis=1, tiled=True)  40.3 us
    all_gather x1, blocking collectives, on_device(): lax.all_gather(w_key, 'sp', axis=0, tiled=True)  33.1 us
    all_gather x1, blocking collectives, on_device(): lax.all_gather(value_weight, 'sp', axis=0, tiled=True)  31.1 us
    reduce_scatter x1, waiting for transfers between devices, on_device(): lax.psum_scatter(jnp.dot(features, out_rows, preferred_element_type=jnp.f...  29.6 us
    all_gather x1, waiting for transfers between devices, on_device(): lax.all_gather(normed, 'tp', axis=0, tiled=True)  16.7 us
    all_gather x1, waiting for transfers between devices, on_device(): lax.all_gather(w_query, 'sp', axis=0, tiled=True)  14.2 us
    all_gather x1, waiting for transfers between devices, on_device(): lax.all_gather(w_out_conv, 'sp', axis=1, tiled=True)  10.6 us
  transfers between devices with their start and end apart: 11, of which 6 were waited for; matrix products, arithmetic and copies ran while one was open for 10% of the time, Pallas kernels for 0%

commit v1 on v0

--- a/solution.py
+++ b/solution.py
@@ -1,6 +1,10 @@
+import functools
+
 import jax
 import jax.numpy as jnp
 from jax import lax
+from jax.experimental import pallas as pl
+from jax.experimental.pallas import tpu as pltpu
 from jax.sharding import PartitionSpec as P
 
 WINDOW_REACH = 128
@@ -130,9 +134,413 @@
     return (mixed, log_total)
 
 
+BF = jnp.bfloat16
+F32 = jnp.float32
+
+
+def fused_kernel(
+    n, x_hbm, gain, wval, wgate, wquery, wkv, taps, cbias, ngain, nbias, sink, woc, woa,
+    mixed, logt,
+    tok, nrm, wq, wc, wo, accq, accc, qb, band, glu, filt, stat, feat, part,
+    p1s, p1r, p2s, p2r, own,
+    lsem, tsem, trec, rsem, rrec, hsem, hrec, ssem, srec, asem, arec, bsem, brec,
+):
+    sp = lax.axis_index("sp")
+    t = lax.axis_index("tp")
+    half = n // 2
+    tl, width = x_hbm.shape
+    length = 4 * tl
+    kb = wval.shape[0]
+    chans = wval.shape[1]
+    qwidth = wquery.shape[1]
+    kvw = wkv.shape[1]
+    hd = kvw // 2
+    heads = sink.shape[1]
+    ob = woc.shape[1]
+    reach = WINDOW_REACH
+    y, c = t // 2, t % 2
+    core_peer = y * 2 + 1 - c
+    y_peer = (1 - y) * 2 + c
+    far_peer = (1 - y) * 2 + 1 - c
+    xbit, zpos = sp % 2, sp // 2
+    pos = (1 - xbit) * zpos + xbit * (n - 1 - zpos)
+
+    def at_pos(q):
+        q = (q + 2 * n) % n
+        hi = q // half
+        return (1 - hi) * (2 * q) + hi * (2 * (n - 1 - q) + 1)
+
+    right, left = at_pos(pos + 1), at_pos(pos - 1)
+    nxt, prv = (sp + 1) % n, (sp + n - 1) % n
+
+    def rows(o, size):
+        return pl.ds(pl.multiple_of(o * size, size), size)
+
+    local = [
+        pltpu.make_async_copy(x_hbm, tok.at[rows(t, tl)], lsem.at[0]),
+        pltpu.make_async_copy(wquery, wq.at[rows(sp, kb), pl.ds(0, qwidth)], lsem.at[1]),
+        pltpu.make_async_copy(wkv, wq.at[rows(sp, kb), pl.ds(qwidth, kvw)], lsem.at[2]),
+        pltpu.make_async_copy(wval, wc.at[rows(sp, kb), pl.ds(0, chans)], lsem.at[3]),
+        pltpu.make_async_copy(wgate, wc.at[rows(sp, kb), pl.ds(chans, chans)], lsem.at[4]),
+        pltpu.make_async_copy(woc, wo.at[sp, pl.ds(0, chans)], lsem.at[5]),
+        pltpu.make_async_copy(woa, wo.at[sp, pl.ds(chans, qwidth)], lsem.at[6]),
+    ]
+    for cp in local:
+        cp.start()
+    barrier = pltpu.get_barrier_semaphore()
+    for dev in (right, left, nxt, prv):
+        pl.semaphore_signal(
+            barrier, inc=1, device_id={"sp": dev}, device_id_type=pl.DeviceIdType.MESH
+        )
+    for dev in (core_peer, y_peer, far_peer):
+        pl.semaphore_signal(
+            barrier, inc=1, device_id={"tp": dev}, device_id_type=pl.DeviceIdType.MESH
+        )
+    pl.semaphore_wait(barrier, 7)
+
+    sent = []
+
+    def remote(src, dst, ss, rs, dev):
+        cp = pltpu.make_async_remote_copy(
+            src_ref=src, dst_ref=dst, send_sem=ss, recv_sem=rs, device_id=dev,
+            device_id_type=pl.DeviceIdType.MESH,
+        )
+        cp.start()
+        sent.append(cp)
+        return cp
+
+    ring = {}
+
+    def block_ref(k, o, h):
+        if k == 0:
+            return wq.at[pl.ds(pl.multiple_of(o * kb + h * (kb // 2), kb // 2), kb // 2)]
+        if k == 1:
+            return wc.at[pl.ds(pl.multiple_of(o * kb + h * (kb // 2), kb // 2), kb // 2)]
+        depth = wo.shape[1] // 2
+        return wo.at[o, pl.ds(h * depth, depth)]
+
+    def ring_event(k, s):
+        for h in (0, 1):
+            for d in (0, 1):
+                if s > 1:
+                    ring[k, d, s - 1, h].wait_recv()
+                if s < half or h == d:
+                    o = at_pos(pos - (s - 1) if d == 0 else pos + (s - 1))
+                    ref = block_ref(k, o, h)
+                    ring[k, d, s, h] = remote(
+                        ref, ref, rsem.at[k, d, s - 1, h], rrec.at[k, d, s - 1, h],
+                        {"sp": right if d == 0 else left},
+                    )
+
+    def ring_last(k):
+        for d in (0, 1):
+            ring[k, d, half, d].wait_recv()
+
+    def owners(s):
+        if s == 0:
+            return [sp]
+        if s == half:
+            return [at_pos(pos + half)]
+        return [at_pos(pos - s), at_pos(pos + s)]
+
+    local[1].wait()
+    local[2].wait()
+    ring_event(0, 1)
+    local[0].wait()
+    hl = tl // 2
+    tokcp = {}
+
+    def tok_send(slot, h, e, dev):
+        ref = tok.at[pl.ds(pl.multiple_of(slot * tl + h * hl, hl), hl)]
+        tokcp[e, h] = remote(ref, ref, tsem.at[e, h], trec.at[e, h], {"tp": dev})
+
+    for h in (0, 1):
+        tok_send(t, h, 0, y_peer)
+    for h in (0, 1):
+        tok_send(t, h, 1, core_peer)
+    for cp in local[3:]:
+        cp.wait()
+
+    def norm_rows(slot):
+        step = 32
+
+        def body(i, carry):
+            r = pl.ds(pl.multiple_of(slot * tl + i * step, step), step)
+            flt = tok[r, :].astype(F32)
+            scale = lax.rsqrt(jnp.mean(flt * flt, axis=-1, keepdims=True) + 1e-06)
+            nrm[r, :] = (flt * scale * gain[...]).astype(BF)
+            return carry
+
+        lax.fori_loop(0, tl // step, body, 0)
+
+    norm_rows(t)
+    for h in (0, 1):
+        tokcp[1, h].wait_recv()
+    norm_rows(core_peer)
+    ring_event(0, 2)
+    for h in (0, 1):
+        tokcp[0, h].wait_recv()
+        tok_send(y_peer, h, 2, core_peer)
+        if h == 0:
+            ring_event(0, 3)
+    norm_rows(y_peer)
+    ring_event(0, 4) if half >= 4 else None
+    ring_event(1, 1)
+    for h in (0, 1):
+        tokcp[2, h].wait_recv()
+    norm_rows(far_peer)
+
+    def project(acc, w, o, first):
+        res = jnp.dot(
+            nrm[:, pl.ds(pl.multiple_of(o * kb, kb), kb)], w[rows(o, kb), :],
+            preferred_element_type=F32,
+        )
+        acc[...] = res if first else acc[...] + res
+
+    def project_all(acc, w):
+        project(acc, w, 0, True)
+
+        def body(o, carry):
+            project(acc, w, o, False)
+            return carry
+
+        lax.fori_loop(1, n, body, 0)
+
+    ring_last(0)
+    project_all(accq, wq)
+    qb[...] = accq[:, 0:qwidth].astype(BF)
+    band[pl.ds(reach, length), :] = accq[:, qwidth : qwidth + kvw].astype(BF)
+    kv_up = remote(
+        band.at[pl.ds(length, reach)], band.at[pl.ds(0, reach)], hsem.at[0], hrec.at[0],
+        {"sp": nxt},
+    )
+    kv_down = remote(
+        band.at[pl.ds(reach, reach)], band.at[pl.ds(length + reach, reach)], hsem.at[1],
+        hrec.at[1], {"sp": prv},
+    )
+    seq_len = length * n
+
+    def attend(b):
+        blk = reach
+        span = blk + 2 * reach
+        kk = band[pl.ds(b * blk, span), 0:hd]
+        vv = band[pl.ds(b * blk, span), hd:kvw]
+        ri = lax.broadcasted_iota(jnp.int32, (blk, span), 0)
+        ci = lax.broadcasted_iota(jnp.int32, (blk, span), 1)
+        kp = sp * length + b * blk - reach + ci
+        valid = (ci >= ri) & (ci <= ri + 2 * reach) & (kp >= 0) & (kp < seq_len)
+        for h in range(heads):
+            q = qb[pl.ds(b * blk, blk), h * hd : (h + 1) * hd]
+            s = lax.dot_general(
+                q, kk, (((1,), (1,)), ((), ())), preferred_element_type=F32
+            ) * hd ** (-0.5)
+            s = jnp.where(valid, s, -1e30)
+            sk = sink[0:1, h : h + 1]
+            top = jnp.maximum(jnp.max(s, axis=-1, keepdims=True), sk)
+            e = jnp.where(valid, jnp.exp(s - top), 0.0)
+            total = jnp.sum(e, axis=-1, keepdims=True) + jnp.exp(sk - top)
+            p = (e * (1.0 / total)).astype(BF)
+            a = jnp.dot(p, vv, preferred_element_type=F32).astype(BF)
+            feat[pl.ds(b * blk, blk), chans + h * hd : chans + (h + 1) * hd] = a
+            logt[pl.ds(b * blk, blk), h : h + 1] = top + jnp.log(total)
+
+    nblk = length // reach
+    ring_event(1, 2)
+    for b in range(1, nblk - 1):
+        attend(b)
+    ring_event(1, 3)
+    kv_up.wait_recv()
+    kv_down.wait_recv()
+    attend(0)
+    attend(nblk - 1)
+    ring_event(1, 4)
+    ring_event(2, 1)
+    ring_last(1)
+    project_all(accc, wc)
+    pad = 16
+    glu[pl.ds(pad, length), :] = (
+        (accc[:, 0:chans] * jax.nn.sigmoid(accc[:, chans : 2 * chans])).astype(BF).astype(F32)
+    )
+    g_up = remote(
+        glu.at[pl.ds(length, pad)], glu.at[pl.ds(0, pad)], hsem.at[2], hrec.at[2], {"sp": nxt}
+    )
+    g_down = remote(
+        glu.at[pl.ds(pad, pad)], glu.at[pl.ds(length + pad, pad)], hsem.at[3], hrec.at[3],
+        {"sp": prv},
+    )
+    ring_event(2, 2)
+    g_up.wait_recv()
+    g_down.wait_recv()
+
+    @pl.when(sp == 0)
+    def _():
+        glu[pl.ds(0, pad), :] = jnp.zeros((pad, chans), F32)
+
+    @pl.when(sp == n - 1)
+    def _():
+        glu[pl.ds(length + pad, pad), :] = jnp.zeros((pad, chans), F32)
+
+    ntaps = taps.shape[0]
+    off = pad - ntaps // 2
+    cstep = 64
+
+    def conv_rows(r0):
+        acc = jnp.zeros((cstep, chans), F32) + cbias[...]
+        for j in range(ntaps):
+            acc = acc + glu[pl.ds(r0 + off + j, cstep), :] * taps[pl.ds(j, 1), :]
+        filt[pl.ds(r0, cstep), :] = acc
+
+    for i in range(length // cstep):
+        conv_rows(i * cstep)
+    lane = lax.broadcasted_iota(jnp.int32, (128, 128), 1)
+    for b in range(length // 128):
+        f = filt[pl.ds(b * 128, 128), :]
+        s1 = jnp.sum(f, axis=-1, keepdims=True)
+        s2 = jnp.sum(f * f, axis=-1, keepdims=True)
+        tile = jnp.where(lane == 0, s1, jnp.where(lane == 1, s2, 0.0))
+        stat[pl.ds(t, 1), :, pl.ds(b * 128, 128)] = jnp.transpose(tile)[None, 0:8, :]
+    scp = []
+    for e, dev in enumerate((y_peer, far_peer, core_peer)):
+        scp.append(remote(stat.at[t], stat.at[t], ssem.at[e], srec.at[e], {"tp": dev}))
+    ring_event(2, 3)
+    for cp in scp:
+        cp.wait_recv()
+    count = chans * 4
+    for b in range(length // 128):
+        cols = pl.ds(b * 128, 128)
+        tot = (stat[0, :, cols] + stat[1, :, cols] + stat[2, :, cols] + stat[3, :, cols]) / count
+        tt = jnp.transpose(jnp.concatenate([tot] * 16, axis=0))
+        center = tt[:, 0:1]
+        spread = tt[:, 1:2] - center * center
+        u = (filt[pl.ds(b * 128, 128), :] - center) * lax.rsqrt(spread + 1e-05)
+        u = u * ngain[...] + nbias[...]
+        feat[pl.ds(b * 128, 128), 0:chans] = (u * jax.nn.sigmoid(u)).astype(BF)
+
+    acp, bcp = {}, {}
+    order = []
+
+    def emit(o):
+        i = len(order)
+        order.append(o)
+        part[...] = jnp.dot(feat[...], wo[o], preferred_element_type=F32)
+        p1s[i, pl.ds(0, tl), :] = part[rows(core_peer, tl), :].astype(BF)
+        p1s[i, pl.ds(tl, tl), :] = part[rows(far_peer, tl), :].astype(BF)
+        acp[i] = remote(p1s.at[i], p1r.at[i], asem.at[i], arec.at[i], {"tp": core_peer})
+        own[i, pl.ds(0, tl), :] = part[rows(t, tl), :]
+        own[i, pl.ds(tl, tl), :] = part[rows(y_peer, tl), :]
+
+    def cross(i):
+        acp[i].wait_recv()
+        p2s[i] = (own[i, pl.ds(tl, tl), :] + p1r[i, pl.ds(tl, tl), :].astype(F32)).astype(BF)
+        bcp[i] = remote(p2s.at[i], p2r.at[i], bsem.at[i], brec.at[i], {"tp": y_peer})
+
+    def finish(i):
+        bcp[i].wait_recv()
+        mixed[:, rows(order[i], ob)] = (
+            own[i, pl.ds(0, tl), :] + p1r[i, pl.ds(0, tl), :].astype(F32)
+            + p2r[i].astype(F32)
+        ).astype(BF)
+
+    def out_step(s):
+        for o in owners(s):
+            emit(o)
+            if len(order) >= 2:
+                cross(len(order) - 2)
+
+    for s in range(half - 1):
+        out_step(s)
+    ring_event(2, 4)
+    out_step(half - 1)
+    ring_last(2)
+    out_step(half)
+    cross(n - 1)
+    for i in range(n):
+        finish(i)
+    for cp in sent:
+        cp.wait_send()
+
+
+def layer(
+    n, parts, tokens, in_gain, w_conv_val, w_conv_gate, w_query, w_key, value_weight, conv_taps,
+    conv_bias, norm_gain, norm_bias, head_sink_logit, w_out_conv, w_out_attn,
+):
+    tl, width = tokens.shape
+    kb, chans = w_conv_val.shape
+    qwidth = w_query.shape[1]
+    kvw = 2 * w_key.shape[1]
+    heads = head_sink_logit.shape[0]
+    ob = w_out_conv.shape[1]
+    fits = (
+        parts == 4 and n == 8 and tl % 128 == 0 and kb % 128 == 0 and ob % 128 == 0
+        and chans % 128 == 0 and kvw == 128 and qwidth == heads * kvw // 2
+        and conv_taps.shape[0] <= 33
+    )
+    if not fits:
+        return on_device(
+            tokens, in_gain, w_conv_val, w_conv_gate, w_query, w_key, value_weight, conv_taps,
+            conv_bias, norm_gain, norm_bias, head_sink_logit, w_out_conv, w_out_attn,
+        )
+    length = 4 * tl
+    half = n // 2
+    wkv = jnp.concatenate([w_key, value_weight], axis=1)
+    vm = pl.BlockSpec(memory_space=pltpu.VMEM)
+    hb = pl.BlockSpec(memory_space=pl.ANY)
+    dma = pltpu.SemaphoreType.DMA
+    return pl.pallas_call(
+        functools.partial(fused_kernel, n),
+        out_shape=(
+            jax.ShapeDtypeStruct((tl, width), BF),
+            jax.ShapeDtypeStruct((length, heads), F32),
+        ),
+        in_specs=[hb, vm, hb, hb, hb, hb, vm, vm, vm, vm, vm, hb, hb],
+        out_specs=(vm, vm),
+        scratch_shapes=[
+            pltpu.VMEM((length, width), BF),
+            pltpu.VMEM((length, width), BF),
+            pltpu.VMEM((n * kb, qwidth + kvw), BF),
+            pltpu.VMEM((n * kb, 2 * chans), BF),
+            pltpu.VMEM((n, chans + qwidth, ob), BF),
+            pltpu.VMEM((length, qwidth + kvw), F32),
+            pltpu.VMEM((length, 2 * chans), F32),
+            pltpu.VMEM((length, qwidth), BF),
+            pltpu.VMEM((length + 2 * WINDOW_REACH, kvw), BF),
+            pltpu.VMEM((length + 32, chans), F32),
+            pltpu.VMEM((length, chans), F32),
+            pltpu.VMEM((4, 8, length), F32),
+            pltpu.VMEM((length, chans + qwidth), BF),
+            pltpu.VMEM((length, ob), F32),
+            pltpu.VMEM((n, 2 * tl, ob), BF),
+            pltpu.VMEM((n, 2 * tl, ob), BF),
+            pltpu.VMEM((n, tl, ob), BF),
+            pltpu.VMEM((n, tl, ob), BF),
+            pltpu.VMEM((n, 2 * tl, ob), F32),
+            dma((7,)),
+            dma((3, 2)),
+            dma((3, 2)),
+            dma((3, 2, half, 2)),
+            dma((3, 2, half, 2)),
+            dma((4,)),
+            dma((4,)),
+            dma((3,)),
+            dma((3,)),
+            dma((n,)),
+            dma((n,)),
+            dma((n,)),
+            dma((n,)),
+        ],
+        compiler_params=pltpu.CompilerParams(
+            collective_id=0, has_side_effects=True, vmem_limit_bytes=56 * 1024 * 1024
+        ),
+    )(
+        tokens, in_gain.reshape(1, width), w_conv_val, w_conv_gate, w_query, wkv, conv_taps,
+        conv_bias.reshape(1, chans), norm_gain.reshape(1, chans), norm_bias.reshape(1, chans),
+        head_sink_logit.reshape(1, heads), w_out_conv, w_out_attn,
+    )
+
+
 def solution(mesh):
     return jax.shard_map(
-        on_device,
+        functools.partial(layer, mesh.shape["sp"], mesh.shape["tp"]),
         mesh=mesh,
         in_specs=(
             P(("sp", "tp"), None),

time: 284 us -> 83.4 us (0.29)
  waiting for transfers between devices: 156 us -> 0 us
  Pallas kernels: 0 us -> 77.2 us
  blocking collectives: 70.5 us -> 0 us
  between operations: 14.4 us -> 0.66 us
  matrix products: 12.5 us -> 0 us
  starting transfers between devices: 10.8 us -> 0 us
  other arithmetic: 9.74 us -> 0.73 us
  local copies, waits for them, and re-layouts: 9.6 us -> 4.54 us
    all_gather x6 -> x0, waiting for transfers between devices: 123 us -> none  [the longest x1 41.2 us: on_device(): lax.all_gather(w_conv_val, 'sp', axis=0, tiled=True)]
    pallas_call x0 -> x1, Pallas kernels: none -> 77.2 us  [layer(): pl.pallas_call(functools.partial(fused_kernel, n), out_shape=(jax.ShapeDt...]
    all_gather x2 -> x0, blocking collectives: 64.2 us -> none  [the longest x1 33.1 us: on_device(): lax.all_gather(w_key, 'sp', axis=0, tiled=True)]
    reduce_scatter x1 -> x0, waiting for transfers between devices: 29.6 us -> none  [on_device(): lax.psum_scatter(jnp.dot(features, out_rows, preferred_element_type=jnp.f...]
    dot_general x4 -> x0, matrix products: 12.5 us -> none  [the longest x1 5 us: on_device(): jnp.dot(lax.all_gather(normed, 'tp', axis=0, tiled=True), joined, preferr...]
    ppermute x4 -> x0, starting transfers between devices: 10.5 us -> none  [the longest x2 7.92 us: with_halo(): lax.ppermute(tail, axis, [(i, (i + 1) % count) for i in range(ends)])]
    concatenate x1 -> x0, local copies, waits for them, and re-layouts: 6.62 us -> none  [on_device(): jnp.concatenate([val_full, gate_full, query_full, key_full, value_full],...]
    psum x1 -> x0, blocking collectives: 6.26 us -> none  [on_device(): lax.psum((jnp.sum(filtered, axis=-1), jnp.sum(filtered * filtered, axis=-...]
  transfers between devices with their start and end apart: 11 -> 0, of which waited for: 6 -> 0; matrix products, arithmetic and copies ran while one was open for 10% -> 0% of each run, Pallas kernels for 0% -> 0%
where the time goes in v1:
time: 83.4 us; the launch traced here: 83.1 us
  Pallas kernels  77.2 us (93%)
  local copies, waits for them, and re-layouts  4.54 us (5%)
    pallas_call x1, Pallas kernels, layer(): pl.pallas_call(functools.partial(fused_kernel, n), out_shape=(jax.ShapeDt...  77.2 us
    unnamed x5, local copies, waits for them, and re-layouts  2.87 us

profile of v1, /device:TPU:0, one launch (start us, length us, event | category | flops | bytes accessed | tf_op | source)
XLA Modules:
  0.0 83.1 jit_solution(8898176812243636881)
XLA Ops:
  0.6 0.0 copy-start
  0.6 0.9 %copy.16 = bf16[256,64]{1,0:T(8,128)(2,1)S(1)} copy(bf16[256,64]{0,1:T(8,128)(2,1)} %param.19) | data formatting | bytes 65536 | tf_op args[5]
  1.5 0.0 copy-done
  1.5 0.1 copy.17
  1.6 0.7 pad_maximum_fusion.wkv
  2.4 77.2 %shard_map.149 = (bf16[128,2048]{1,0:T(8,128)(2,1)}, f32[512,4]{1,0:T(8,128)}) custom-call(bf16[128,2048]{1,0:T(8,128)(2,1)} %x_hbm.1, f32[1,2048]{1,0:T(1,128)} %bitcast.5, bf16[256,256]{1,0:T(8,128)(2,1)} %wval.1, bf16[256,256]{1,0:T(8,128)(2,1)} %wgate.1, bf16[256,256]{1,0:T(8,128)(2,1)} %wquery.1, bf16[256,128]{1,0:T(8,128)(2,1)} %pad_maximum_fusion.wkv, ...), custom_call_target="tpu_custom_call" | custom-call | tf_op jit(solution)/shard_map/pallas_call | solution.py:489
  79.6 1.7 %copy.18 = f32[512,4]{0,1:T(4,128)} copy(f32[512,4]{1,0:T(8,128)} %get-tuple-element.3) | data formatting | bytes 16384 | tf_op jit(solution)/shard_map/pallas_call | solution.py:489
  81.2 1.9 %copy.20 = bf16[128,2048]{1,0:T(8,128)(2,1)} copy(bf16[128,2048]{1,0:T(8,128)(2,1)} %get-tuple-element.6) | data formatting | bytes 1048576
Async XLA Ops:
  0.6 0.9 %copy-start = (bf16[256,64]{0,1:T(8,128)(2,1)S(1)}, bf16[256,64]{0,1:T(8,128)(2,1)}, u32[]{:S(2)}) copy-start(bf16[256,64]{0,1:T(8,128)(2,1)} %param.20) | copy-start | bytes 98308

commit v2 on v1

--- a/solution.py
+++ b/solution.py
@@ -139,7 +139,7 @@
 
 
 def fused_kernel(
-    n, x_hbm, gain, wval, wgate, wquery, wkv, taps, cbias, ngain, nbias, sink, woc, woa,
+    n, x_hbm, gain, wval, wgate, wquery, wkey, wvalue, taps, cbias, ngain, nbias, sink, woc, woa,
     mixed, logt,
     tok, nrm, wq, wc, wo, accq, accc, qb, band, glu, filt, stat, feat, part,
     p1s, p1r, p2s, p2r, own,
@@ -153,8 +153,8 @@
     kb = wval.shape[0]
     chans = wval.shape[1]
     qwidth = wquery.shape[1]
-    kvw = wkv.shape[1]
-    hd = kvw // 2
+    hd = wkey.shape[0]
+    kvw = 2 * hd
     heads = sink.shape[1]
     ob = woc.shape[1]
     reach = WINDOW_REACH
@@ -178,8 +178,9 @@
 
     local = [
         pltpu.make_async_copy(x_hbm, tok.at[rows(t, tl)], lsem.at[0]),
-        pltpu.make_async_copy(wquery, wq.at[rows(sp, kb), pl.ds(0, qwidth)], lsem.at[1]),
-        pltpu.make_async_copy(wkv, wq.at[rows(sp, kb), pl.ds(qwidth, kvw)], lsem.at[2]),
+        pltpu.make_async_copy(wquery, wq.at[sp, pl.ds(0, kb)], lsem.at[1]),
+        pltpu.make_async_copy(wkey, wq.at[sp, pl.ds(kb, hd)], lsem.at[2]),
+        pltpu.make_async_copy(wvalue, wq.at[sp, pl.ds(kb + hd, hd)], lsem.at[7]),
         pltpu.make_async_copy(wval, wc.at[rows(sp, kb), pl.ds(0, chans)], lsem.at[3]),
         pltpu.make_async_copy(wgate, wc.at[rows(sp, kb), pl.ds(chans, chans)], lsem.at[4]),
         pltpu.make_async_copy(woc, wo.at[sp, pl.ds(0, chans)], lsem.at[5]),
@@ -213,14 +214,15 @@
 
     def block_ref(k, o, h):
         if k == 0:
-            return wq.at[pl.ds(pl.multiple_of(o * kb + h * (kb // 2), kb // 2), kb // 2)]
+            depth = wq.shape[1] // 2
+            return wq.at[o, pl.ds(h * depth, depth)]
         if k == 1:
             return wc.at[pl.ds(pl.multiple_of(o * kb + h * (kb // 2), kb // 2), kb // 2)]
         depth = wo.shape[1] // 2
         return wo.at[o, pl.ds(h * depth, depth)]
 
-    def ring_event(k, s):
-        for h in (0, 1):
+    def ring_event(k, s, halves=(0, 1)):
+        for h in halves:
             for d in (0, 1):
                 if s > 1:
                     ring[k, d, s - 1, h].wait_recv()
@@ -243,9 +245,9 @@
             return [at_pos(pos + half)]
         return [at_pos(pos - s), at_pos(pos + s)]
 
-    local[1].wait()
-    local[2].wait()
-    ring_event(0, 1)
+    local[4].wait()
+    local[5].wait()
+    ring_event(1, 1)
     local[0].wait()
     hl = tl // 2
     tokcp = {}
@@ -258,8 +260,8 @@
         tok_send(t, h, 0, y_peer)
     for h in (0, 1):
         tok_send(t, h, 1, core_peer)
-    for cp in local[3:]:
-        cp.wait()
+    for i in (1, 2, 3, 6, 7):
+        local[i].wait()
 
     def norm_rows(slot):
         step = 32
@@ -276,38 +278,124 @@
     norm_rows(t)
     for h in (0, 1):
         tokcp[1, h].wait_recv()
+    ring_event(1, 2, (0,))
     norm_rows(core_peer)
-    ring_event(0, 2)
-    for h in (0, 1):
-        tokcp[0, h].wait_recv()
-        tok_send(y_peer, h, 2, core_peer)
-        if h == 0:
-            ring_event(0, 3)
+    ring_event(1, 2, (1,))
+    tokcp[0, 0].wait_recv()
+    tok_send(y_peer, 0, 2, core_peer)
+    ring_event(1, 3, (0,))
+    ring_event(1, 3, (1,))
+    tokcp[0, 1].wait_recv()
+    tok_send(y_peer, 1, 2, core_peer)
+    ring_event(0, 1, (0,))
     norm_rows(y_peer)
-    ring_event(0, 4) if half >= 4 else None
-    ring_event(1, 1)
     for h in (0, 1):
         tokcp[2, h].wait_recv()
     norm_rows(far_peer)
 
-    def project(acc, w, o, first):
-        res = jnp.dot(
-            nrm[:, pl.ds(pl.multiple_of(o * kb, kb), kb)], w[rows(o, kb), :],
-            preferred_element_type=F32,
-        )
-        acc[...] = res if first else acc[...] + res
-
-    def project_all(acc, w):
-        project(acc, w, 0, True)
-
-        def body(o, carry):
-            project(acc, w, o, False)
-            return carry
-
-        lax.fori_loop(1, n, body, 0)
-
+    def columns(o):
+        return nrm[:, pl.ds(pl.multiple_of(o * kb, kb), kb)]
+
+    def project_conv(s):
+        for o in owners(s):
+            res = jnp.dot(columns(o), wc[rows(o, kb), :], preferred_element_type=F32)
+            accc[...] = res if s == 0 else accc[...] + res
+
+    def project_heads(s):
+        for o in owners(s):
+            lhs = columns(o)
+            res = jnp.dot(lhs, wq[o, 0:kb, :], preferred_element_type=F32)
+            two = lax.dot_general(
+                lhs, wq[o, kb : kb + kvw, :], (((1,), (1,)), ((), ())),
+                preferred_element_type=F32,
+            )
+            if s == 0:
+                accq[:, 0:qwidth] = res
+                accq[:, qwidth : qwidth + kvw] = two
+            else:
+                accq[:, 0:qwidth] = accq[:, 0:qwidth] + res
+                accq[:, qwidth : qwidth + kvw] = accq[:, qwidth : qwidth + kvw] + two
+
+    project_conv(0)
+    ring_event(1, 4)
+    ring_event(0, 1, (1,))
+    project_conv(1)
+    project_conv(2)
+    project_conv(3)
+    ring_event(0, 2, (0,))
+    ring_last(1)
+    project_conv(4)
+    pad = 16
+    glu[pl.ds(pad, length), :] = (
+        (accc[:, 0:chans] * jax.nn.sigmoid(accc[:, chans : 2 * chans])).astype(BF).astype(F32)
+    )
+    g_up = remote(
+        glu.at[pl.ds(length, pad)], glu.at[pl.ds(0, pad)], hsem.at[2], hrec.at[2], {"sp": nxt}
+    )
+    g_down = remote(
+        glu.at[pl.ds(pad, pad)], glu.at[pl.ds(length + pad, pad)], hsem.at[3], hrec.at[3],
+        {"sp": prv},
+    )
+    ring_event(0, 2, (1,))
+    ntaps = taps.shape[0]
+    off = pad - ntaps // 2
+    cstep = 64
+
+    def conv_rows(r0):
+        acc = jnp.zeros((cstep, chans), F32) + cbias[...]
+        for j in range(ntaps):
+            acc = acc + glu[pl.ds(r0 + off + j, cstep), :] * taps[pl.ds(j, 1), :]
+        filt[pl.ds(r0, cstep), :] = acc
+
+    nconv = length // cstep
+    for i in range(1, nconv - 1):
+        conv_rows(i * cstep)
+    ring_event(0, 3)
+    g_up.wait_recv()
+    g_down.wait_recv()
+
+    @pl.when(sp == 0)
+    def _():
+        glu[pl.ds(0, pad), :] = jnp.zeros((pad, chans), F32)
+
+    @pl.when(sp == n - 1)
+    def _():
+        glu[pl.ds(length + pad, pad), :] = jnp.zeros((pad, chans), F32)
+
+    conv_rows(0)
+    conv_rows((nconv - 1) * cstep)
+    lane = lax.broadcasted_iota(jnp.int32, (128, 128), 1)
+    for b in range(length // 128):
+        f = filt[pl.ds(b * 128, 128), :]
+        s1 = jnp.sum(f, axis=-1, keepdims=True)
+        s2 = jnp.sum(f * f, axis=-1, keepdims=True)
+        tile = jnp.where(lane == 0, s1, jnp.where(lane == 1, s2, 0.0))
+        stat[pl.ds(t, 1), :, pl.ds(b * 128, 128)] = jnp.transpose(tile)[None, 0:8, :]
+    scp = []
+    for e, dev in enumerate((y_peer, far_peer, core_peer)):
+        scp.append(remote(stat.at[t], stat.at[t], ssem.at[e], srec.at[e], {"tp": dev}))
+    ring_event(2, 1, (0,))
+    ring_event(0, 4)
+    ring_event(2, 1, (1,))
+    project_heads(0)
+    project_heads(1)
+    project_heads(2)
+    for cp in scp:
+        cp.wait_recv()
+    count = chans * 4
+    for b in range(length // 128):
+        cols = pl.ds(b * 128, 128)
+        tot = (stat[0, :, cols] + stat[1, :, cols] + stat[2, :, cols] + stat[3, :, cols]) / count
+        tt = jnp.transpose(jnp.concatenate([tot] * 16, axis=0))
+        center = tt[:, 0:1]
+        spread = tt[:, 1:2] - center * center
+        u = (filt[pl.ds(b * 128, 128), :] - center) * lax.rsqrt(spread + 1e-05)
+        u = u * ngain[...] + nbias[...]
+        feat[pl.ds(b * 128, 128), 0:chans] = (u * jax.nn.sigmoid(u)).astype(BF)
+
+    project_heads(3)
     ring_last(0)
-    project_all(accq, wq)
+    project_heads(4)
     qb[...] = accq[:, 0:qwidth].astype(BF)
     band[pl.ds(reach, length), :] = accq[:, qwidth : qwidth + kvw].astype(BF)
     kv_up = remote(
@@ -329,6 +417,7 @@
         ci = lax.broadcasted_iota(jnp.int32, (blk, span), 1)
         kp = sp * length + b * blk - reach + ci
         valid = (ci >= ri) & (ci <= ri + 2 * reach) & (kp >= 0) & (kp < seq_len)
+        logs = []
         for h in range(heads):
             q = qb[pl.ds(b * blk, blk), h * hd : (h + 1) * hd]
             s = lax.dot_general(
@@ -342,79 +431,20 @@
             p = (e * (1.0 / total)).astype(BF)
             a = jnp.dot(p, vv, preferred_element_type=F32).astype(BF)
             feat[pl.ds(b * blk, blk), chans + h * hd : chans + (h + 1) * hd] = a
-            logt[pl.ds(b * blk, blk), h : h + 1] = top + jnp.log(total)
+            logs.append(top + jnp.log(total))
+        wide = jnp.zeros((blk, 128), F32)
+        for h in range(heads):
+            wide = jnp.where(lane == h, logs[h], wide)
+        logt[:, pl.ds(b * blk, blk)] = jnp.transpose(wide)[0:heads, :]
 
     nblk = length // reach
-    ring_event(1, 2)
     for b in range(1, nblk - 1):
         attend(b)
-    ring_event(1, 3)
+    ring_event(2, 2)
     kv_up.wait_recv()
     kv_down.wait_recv()
     attend(0)
     attend(nblk - 1)
-    ring_event(1, 4)
-    ring_event(2, 1)
-    ring_last(1)
-    project_all(accc, wc)
-    pad = 16
-    glu[pl.ds(pad, length), :] = (
-        (accc[:, 0:chans] * jax.nn.sigmoid(accc[:, chans : 2 * chans])).astype(BF).astype(F32)
-    )
-    g_up = remote(
-        glu.at[pl.ds(length, pad)], glu.at[pl.ds(0, pad)], hsem.at[2], hrec.at[2], {"sp": nxt}
-    )
-    g_down = remote(
-        glu.at[pl.ds(pad, pad)], glu.at[pl.ds(length + pad, pad)], hsem.at[3], hrec.at[3],
-        {"sp": prv},
-    )
-    ring_event(2, 2)
-    g_up.wait_recv()
-    g_down.wait_recv()
-
-    @pl.when(sp == 0)
-    def _():
-        glu[pl.ds(0, pad), :] = jnp.zeros((pad, chans), F32)
-
-    @pl.when(sp == n - 1)
-    def _():
-        glu[pl.ds(length + pad, pad), :] = jnp.zeros((pad, chans), F32)
-
-    ntaps = taps.shape[0]
-    off = pad - ntaps // 2
-    cstep = 64
-
-    def conv_rows(r0):
-        acc = jnp.zeros((cstep, chans), F32) + cbias[...]
-        for j in range(ntaps):
-            acc = acc + glu[pl.ds(r0 + off + j, cstep), :] * taps[pl.ds(j, 1), :]
-        filt[pl.ds(r0, cstep), :] = acc
-
-    for i in range(length // cstep):
-        conv_rows(i * cstep)
-    lane = lax.broadcasted_iota(jnp.int32, (128, 128), 1)
-    for b in range(length // 128):
-        f = filt[pl.ds(b * 128, 128), :]
-        s1 = jnp.sum(f, axis=-1, keepdims=True)
-        s2 = jnp.sum(f * f, axis=-1, keepdims=True)
-        tile = jnp.where(lane == 0, s1, jnp.where(lane == 1, s2, 0.0))
-        stat[pl.ds(t, 1), :, pl.ds(b * 128, 128)] = jnp.transpose(tile)[None, 0:8, :]
-    scp = []
-    for e, dev in enumerate((y_peer, far_peer, core_peer)):
-        scp.append(remote(stat.at[t], stat.at[t], ssem.at[e], srec.at[e], {"tp": dev}))
-    ring_event(2, 3)
-    for cp in scp:
-        cp.wait_recv()
-    count = chans * 4
-    for b in range(length // 128):
-        cols = pl.ds(b * 128, 128)
-        tot = (stat[0, :, cols] + stat[1, :, cols] + stat[2, :, cols] + stat[3, :, cols]) / count
-        tt = jnp.transpose(jnp.concatenate([tot] * 16, axis=0))
-        center = tt[:, 0:1]
-        spread = tt[:, 1:2] - center * center
-        u = (filt[pl.ds(b * 128, 128), :] - center) * lax.rsqrt(spread + 1e-05)
-        u = u * ngain[...] + nbias[...]
-        feat[pl.ds(b * 128, 128), 0:chans] = (u * jax.nn.sigmoid(u)).astype(BF)
 
     acp, bcp = {}, {}
     order = []
@@ -447,15 +477,21 @@
             if len(order) >= 2:
                 cross(len(order) - 2)
 
-    for s in range(half - 1):
-        out_step(s)
+    out_step(0)
+    ring_event(2, 3)
+    out_step(1)
+    out_step(2)
     ring_event(2, 4)
-    out_step(half - 1)
+    out_step(3)
+    for i in range(n - 4):
+        finish(i)
     ring_last(2)
     out_step(half)
+    for i in range(n - 4, n - 2):
+        finish(i)
     cross(n - 1)
-    for i in range(n):
-        finish(i)
+    finish(n - 2)
+    finish(n - 1)
     for cp in sent:
         cp.wait_send()
 
@@ -472,7 +508,7 @@
     ob = w_out_conv.shape[1]
     fits = (
         parts == 4 and n == 8 and tl % 128 == 0 and kb % 128 == 0 and ob % 128 == 0
-        and chans % 128 == 0 and kvw == 128 and qwidth == heads * kvw // 2
+        and chans % 128 == 0 and kvw == 128 and kb == qwidth and qwidth == heads * kvw // 2
         and conv_taps.shape[0] <= 33
     )
     if not fits:
@@ -482,22 +518,21 @@
         )
     length = 4 * tl
     half = n // 2
-    wkv = jnp.concatenate([w_key, value_weight], axis=1)
     vm = pl.BlockSpec(memory_space=pltpu.VMEM)
     hb = pl.BlockSpec(memory_space=pl.ANY)
     dma = pltpu.SemaphoreType.DMA
-    return pl.pallas_call(
+    mixed, log_rows = pl.pallas_call(
         functools.partial(fused_kernel, n),
         out_shape=(
             jax.ShapeDtypeStruct((tl, width), BF),
-            jax.ShapeDtypeStruct((length, heads), F32),
+            jax.ShapeDtypeStruct((heads, length), F32),
         ),
-        in_specs=[hb, vm, hb, hb, hb, hb, vm, vm, vm, vm, vm, hb, hb],
+        in_specs=[hb, vm, hb, hb, hb, hb, hb, vm, vm, vm, vm, vm, hb, hb],
         out_specs=(vm, vm),
         scratch_shapes=[
             pltpu.VMEM((length, width), BF),
             pltpu.VMEM((length, width), BF),
-            pltpu.VMEM((n * kb, qwidth + kvw), BF),
+            pltpu.VMEM((n, kb + kvw, qwidth), BF),
             pltpu.VMEM((n * kb, 2 * chans), BF),
             pltpu.VMEM((n, chans + qwidth, ob), BF),
             pltpu.VMEM((length, qwidth + kvw), F32),
@@ -514,7 +549,7 @@
             pltpu.VMEM((n, tl, ob), BF),
             pltpu.VMEM((n, tl, ob), BF),
             pltpu.VMEM((n, 2 * tl, ob), F32),
-            dma((7,)),
+            dma((8,)),
             dma((3, 2)),
             dma((3, 2)),
             dma((3, 2, half, 2)),
@@ -532,10 +567,11 @@
             collective_id=0, has_side_effects=True, vmem_limit_bytes=56 * 1024 * 1024
         ),
     )(
-        tokens, in_gain.reshape(1, width), w_conv_val, w_conv_gate, w_query, wkv, conv_taps,
-        conv_bias.reshape(1, chans), norm_gain.reshape(1, chans), norm_bias.reshape(1, chans),
+        tokens, in_gain.reshape(1, width), w_conv_val, w_conv_gate, w_query, w_key.T, value_weight.T,
+        conv_taps, conv_bias.reshape(1, chans), norm_gain.reshape(1, chans), norm_bias.reshape(1, chans),
         head_sink_logit.reshape(1, heads), w_out_conv, w_out_attn,
     )
+    return mixed, log_rows.T
 
 
 def solution(mesh):

time: 83.4 us -> 78.2 us (0.938)
  Pallas kernels: 77.2 us -> 74.9 us
  local copies, waits for them, and re-layouts: 4.54 us -> 2.49 us
    pallas_call x1, Pallas kernels: 77.2 us -> 74.9 us  [layer(): pl.pallas_call(functools.partial(fused_kernel, n), out_shape=(jax.ShapeDt...]
    pallas_call x1 -> x0, local copies, waits for them, and re-layouts: 1.66 us -> none  [layer(): pl.pallas_call(functools.partial(fused_kernel, n), out_shape=(jax.ShapeDt...]
    unnamed x5 -> x4, local copies, waits for them, and re-layouts: 2.87 us -> 2.49 us
where the time goes in v2:
time: 78.2 us; the launch traced here: 78 us
  Pallas kernels  74.9 us (96%)
  local copies, waits for them, and re-layouts  2.49 us (3%)
    pallas_call x1, Pallas kernels, layer(): pl.pallas_call(functools.partial(fused_kernel, n), out_shape=(jax.ShapeDt...  74.9 us
    unnamed x4, local copies, waits for them, and re-layouts  2.49 us

profile of v2, /device:TPU:0, one launch (start us, length us, event | category | flops | bytes accessed | tf_op | source)
XLA Modules:
  0.0 78.0 jit_solution(3369004278123582707)
XLA Ops:
  0.6 74.9 %shard_map.149 = (bf16[128,2048]{1,0:T(8,128)(2,1)}, f32[4,512]{1,0:T(4,128)}) custom-call(bf16[128,2048]{1,0:T(8,128)(2,1)} %x_hbm.1, f32[1,2048]{1,0:T(1,128)} %bitcast.10, bf16[256,256]{1,0:T(8,128)(2,1)} %wval.1, bf16[256,256]{1,0:T(8,128)(2,1)} %wgate.1, bf16[256,256]{1,0:T(8,128)(2,1)} %wquery.1, bf16[64,256]{1,0:T(8,128)(2,1)} %bitcast.8, ...), custom_call_target="tpu_custom_call" | custom-call | tf_op jit(solution)/shard_map/pallas_call | solution.py:524
  75.5 0.0 copy-start
  75.5 1.9 %copy.18 = bf16[128,2048]{1,0:T(8,128)(2,1)} copy(bf16[128,2048]{1,0:T(8,128)(2,1)} %get-tuple-element.8) | data formatting | bytes 1048576
  77.4 0.0 copy-done
  77.4 0.6 copy.19
Async XLA Ops:
  75.5 1.9 %copy-start = (f32[4,512]{1,0:T(4,128)S(1)}, f32[4,512]{1,0:T(4,128)}, u32[]{:S(2)}) copy-start(f32[4,512]{1,0:T(4,128)} %get-tuple-element.5) | copy-start | bytes 24580

commit v3 on v2

--- a/solution.py
+++ b/solution.py
@@ -438,9 +438,10 @@
         logt[:, pl.ds(b * blk, blk)] = jnp.transpose(wide)[0:heads, :]
 
     nblk = length // reach
-    for b in range(1, nblk - 1):
+    attend(1)
+    ring_event(2, 2)
+    for b in range(2, nblk - 1):
         attend(b)
-    ring_event(2, 2)
     kv_up.wait_recv()
     kv_down.wait_recv()
     attend(0)
@@ -483,15 +484,11 @@
     out_step(2)
     ring_event(2, 4)
     out_step(3)
-    for i in range(n - 4):
-        finish(i)
     ring_last(2)
     out_step(half)
-    for i in range(n - 4, n - 2):
+    cross(n - 1)
+    for i in range(n):
         finish(i)
-    cross(n - 1)
-    finish(n - 2)
-    finish(n - 1)
     for cp in sent:
         cp.wait_send()
 

time: 78.2 us -> 77.6 us (level)
  no operation moved by 1% of the time
where the time goes in v3:
time: 77.6 us; the launch traced here: 77.4 us
  Pallas kernels  74.3 us (96%)
  local copies, waits for them, and re-layouts  2.49 us (3%)
    pallas_call x1, Pallas kernels, layer(): pl.pallas_call(functools.partial(fused_kernel, n), out_shape=(jax.ShapeDt...  74.3 us
    unnamed x4, local copies, waits for them, and re-layouts  2.49 us

profile of v3, /device:TPU:0, one launch (start us, length us, event | category | flops | bytes accessed | tf_op | source)
XLA Modules:
  0.0 77.4 jit_solution(3443548451948539687)
XLA Ops:
  0.6 74.3 %shard_map.149 = (bf16[128,2048]{1,0:T(8,128)(2,1)}, f32[4,512]{1,0:T(4,128)}) custom-call(bf16[128,2048]{1,0:T(8,128)(2,1)} %x_hbm.1, f32[1,2048]{1,0:T(1,128)} %bitcast.10, bf16[256,256]{1,0:T(8,128)(2,1)} %wval.1, bf16[256,256]{1,0:T(8,128)(2,1)} %wgate.1, bf16[256,256]{1,0:T(8,128)(2,1)} %wquery.1, bf16[64,256]{1,0:T(8,128)(2,1)} %bitcast.8, ...), custom_call_target="tpu_custom_call" | custom-call | tf_op jit(solution)/shard_map/pallas_call | solution.py:521
  74.9 0.0 copy-start
  74.9 1.9 %copy.18 = bf16[128,2048]{1,0:T(8,128)(2,1)} copy(bf16[128,2048]{1,0:T(8,128)(2,1)} %get-tuple-element.8) | data formatting | bytes 1048576
  76.8 0.0 copy-done
  76.8 0.6 copy.19
Async XLA Ops:
  74.9 1.9 %copy-start = (f32[4,512]{1,0:T(4,128)S(1)}, f32[4,512]{1,0:T(4,128)}, u32[]{:S(2)}) copy-start(f32[4,512]{1,0:T(4,128)} %get-tuple-element.5) | copy-start | bytes 24580
